TPU v7x, 32 devices: a whole 2x2x4 slice. The times are simulated.
32 devices in a mesh: fs: 8 (over z, y), tp: 4 (over x, core).
Axes of the slice: x: 2, y: 2, z: 4, core: 2. Of those that a mesh axis runs over, the one named last changes fastest.
Arguments:
- tokens: bfloat16 [8192, 2048], P('fs', 'tp'), may hold values from -6 to 6
- norm_gain: float32 [2048], P('fs'), may hold values from 0.1 to 1.9
- up_master: float32 [2048, 8192], P('fs', 'tp'), may hold values from -0.125 to 0.125
- down_master: float32 [2048, 8192], P('fs', 'tp'), may hold values from -0.0625 to 0.0625
Outputs:
- up_weights: bfloat16 [2048, 8192], P(None, 'tp')
- down_weights: bfloat16 [8192, 2048], P('tp')
- mlp_out: bfloat16 [8192, 2048], P('fs', 'tp')
All inputs are finite; a program needn't handle non-finite values.
Results may differ from a plain program's by a relative error of at most 0.014.
Values may be sent and summed in bfloat16 or wider, within the bound.
A program may use at most 128 MiB of HBM per device.

v0:
```python
import jax
import jax.numpy as jnp
from jax import lax
from jax.sharding import PartitionSpec as P

norm_floor = 1e-06


def on_device(tokens, norm_gain, up_master, down_master):
    up_local = (norm_gain[:, None] * up_master).astype(jnp.bfloat16)
    down_local = down_master.astype(jnp.bfloat16)
    gathered = lax.all_gather(tokens, "tp", axis=1, tiled=True)
    widened = gathered.astype(jnp.float32)
    normed = (
        widened * lax.rsqrt(jnp.mean(widened * widened, axis=-1, keepdims=True) + norm_floor)
    ).astype(jnp.bfloat16)
    up_whole, down_whole = (
        lax.all_gather(up_local, "fs", axis=0, tiled=True),
        lax.all_gather(down_local, "fs", axis=0, tiled=True),
    )
    preact = jnp.dot(normed, up_whole, preferred_element_type=jnp.float32)
    hidden = jnp.square(jax.nn.relu(preact)).astype(jnp.bfloat16)
    partial_value = jnp.einsum("tf,df->td", hidden, down_whole, preferred_element_type=jnp.float32)
    summed = lax.psum_scatter(
        partial_value.astype(jnp.bfloat16), "tp", scatter_dimension=1, tiled=True
    )
    return (up_whole, jnp.transpose(down_whole), summed)


def solution(mesh):
    in_specs = (P("fs", "tp"), P("fs"), P("fs", "tp"), P("fs", "tp"))
    out_specs = (P(None, "tp"), P("tp", None), P("fs", "tp"))
    return jax.shard_map(
        on_device, mesh=mesh, in_specs=in_specs, out_specs=out_specs, check_vma=False
    )
```

profile of v0, /device:TPU:0, one launch (start us, length us, event | category | flops | bytes accessed | tf_op | source)
XLA Modules:
  0.0 391.6 jit_solution(10137496696475460250)
XLA Ops:
  7.2 0.0 all-gather.8.cloned.1.call-start
  7.2 0.7 all-gather.8.cloned.1.call-update
  7.9 0.0 all-gather.4.cloned.1.call-start
  7.9 2.7 multiply_convert_fusion.1
  10.7 0.0 all-gather.4.cloned.1.call-update
  10.7 0.0 all-gather.6.cloned.1.call-start
  10.8 2.5 copy.7
  13.3 0.0 all-gather.6.cloned.1.call-update
  13.3 0.0 reduce-scatter.2.cloned.1.call-start
  13.4 33.4 %all-gather.8.cloned.1.call-done = bf16[1024,2048]{1,0:T(8,128)(2,1)} async-done(((bf16[1024,512]{1,0:T(8,128)(2,1)}), bf16[1024,2048]{1,0:T(8,128)(2,1)}) %all-gather.8.cloned.1.call-update) | async-done | bytes 4194320 | tf_op jit(solution)/shard_map/all_gather | solution.py:12
  46.7 3.1 fusion
  49.8 124.1 %all-gather.4.cloned.1.call-done = bf16[2048,2048]{1,0:T(8,128)(2,1)} async-done(((bf16[256,2048]{1,0:T(8,128)(2,1)}), bf16[2048,2048]{1,0:T(8,128)(2,1)}) %all-gather.4.cloned.1.call-update) | async-done | bytes 8388624 | tf_op jit(solution)/shard_map/all_gather | solution.py:18
  174.0 125.8 %all-gather.6.cloned.1.call-done = bf16[2048,2048]{0,1:T(8,128)(2,1)} async-done(((bf16[256,2048]{0,1:T(8,128)(2,1)}), bf16[2048,2048]{0,1:T(8,128)(2,1)}) %all-gather.6.cloned.1.call-update) | async-done | bytes 8388624 | tf_op jit(solution)/shard_map/all_gather | solution.py:19
  299.7 25.7 %fusion.9 = bf16[1024,2048]{1,0:T(8,128)(2,1)} fusion(bf16[2048,2048]{0,1:T(8,128)(2,1)} %all-gather.6.cloned.1.call-done, bf16[2048,2048]{1,0:T(8,128)(2,1)} %all-gather.4.cloned.1.call-done, bf16[1024,2048]{1,0:T(8,128)(2,1)} %all-gather.8.cloned.1.call-done, f32[1024]{0:T(1024)S(1)} %add_rsqrt_fusion), kind=kOutput, calls=%fused_computation.8 | convolution fusion | flops 17194549248 | bytes 25169920 | tf_op jit(solution)/shard_map/tf,df->td/dot_general | solution.py:23
  325.4 0.0 reduce-scatter.2.cloned.1.call-update
  325.5 42.7 %reduce-scatter.2.cloned.1.call-done = bf16[1024,512]{1,0:T(8,128)(2,1)} async-done(((bf16[1024,2048]{1,0:T(8,128)(2,1)}), bf16[1024,512]{1,0:T(8,128)(2,1)}) %reduce-scatter.2.cloned.1.call-update) | async-done | bytes 1048592 | tf_op jit(solution)/shard_map/reduce_scatter | solution.py:24
  368.2 8.4 %copy.10 = bf16[2048,2048]{1,0:T(8,128)(2,1)} copy(bf16[2048,2048]{1,0:T(8,128)(2,1)} %all-gather.4.cloned.1.call-done) | data formatting | bytes 16777216
  376.6 8.4 %copy.11 = bf16[2048,2048]{1,0:T(8,128)(2,1)} copy(bf16[2048,2048]{1,0:T(8,128)(2,1)} %bitcast.3) | data formatting | bytes 16777216
  (1 shorter events, 0.0 us)
Async XLA Ops:
  7.2 39.6 %all-gather.8.cloned.1.call-start = ((), (), s32[]{:S(2)}) async-start(), calls=%async_computation.3 | async-start | bytes 5242880 | tf_op jit(solution)/shard_map/all_gather | solution.py:12
  7.9 166.1 %all-gather.4.cloned.1.call-start = ((), (), s32[]{:S(2)}) async-start(), calls=%async_computation.1 | async-start | bytes 9437184 | tf_op jit(solution)/shard_map/all_gather | solution.py:18
  10.7 289.0 %all-gather.6.cloned.1.call-start = ((), (), s32[]{:S(2)}) async-start(), calls=%async_computation.2 | async-start | bytes 9437184 | tf_op jit(solution)/shard_map/all_gather | solution.py:19
  13.3 354.8 %reduce-scatter.2.cloned.1.call-start = ((), (), s32[]{:S(2)}) async-start(), calls=%async_computation.4 | async-start | bytes 5242880 | tf_op jit(solution)/shard_map/reduce_scatter | solution.py:24
Sparse Core Ops, SparseCore 0:
  9.5 37.1 all-gather.7
  49.4 124.4 all-gather.3
  176.6 123.1 all-gather.5
  325.6 42.5 reduce-scatter.1
where the time goes:
time: 392 us
  waiting for transfers between devices  327 us (83%)
  matrix products  25.7 us (7%)
  local copies, waits for them, and re-layouts  19.4 us (5%)
  between operations  13.8 us (4%)
  other arithmetic  5.82 us (1%)
    all_gather x1, waiting for transfers between devices, on_device(): lax.all_gather(down_local, 'fs', axis=0, tiled=True)  126 us
    all_gather x1, waiting for transfers between devices, on_device(): lax.all_gather(up_local, 'fs', axis=0, tiled=True)  124 us
    reduce_scatter x1, waiting for transfers between devices, on_device(): lax.psum_scatter(partial_value.astype(jnp.bfloat16), 'tp', scatter_dimens...  42.7 us
    all_gather x1, waiting for transfers between devices, on_device(): gathered = lax.all_gather(tokens, 'tp', axis=1, tiled=True)  33.4 us
    dot_general x1, matrix products, on_device(): jnp.einsum('tf,df->td', hidden, down_whole, preferred_element_type=jnp.fl...  25.7 us
    unnamed x3, local copies, waits for them, and re-layouts  19.4 us
  transfers between devices with their start and end apart: 4, of which 4 were waited for; matrix products, arithmetic and copies ran while one was open for 2% of the time, Pallas kernels for 0%

commit v1 on v0

v1 whole, which is shorter than its diff:
```python
import functools

import jax
import jax.numpy as jnp
from jax import lax
from jax.experimental import pallas as pl
from jax.experimental.pallas import tpu as pltpu
from jax.sharding import PartitionSpec as P

norm_floor = 1e-06
MESH = pl.DeviceIdType.MESH


def grid_of(n):
    ny = max(d for d in range(1, n + 1) if n % d == 0 and d * d <= n)
    return n // ny, ny


def position_of(f, nz, ny):
    if ny == 1:
        return f
    z, y = lax.div(f, ny), lax.rem(f, ny)
    tail = lax.div(y + (ny - 1), ny)
    k = nz - 1 - z
    odd = lax.rem(k, 2)
    r = (1 - odd) * (y - 1) + odd * (ny - 1 - y)
    return (1 - tail) * z + tail * (nz + k * (ny - 1) + r)


def index_at(p, nz, ny):
    if ny == 1:
        return p
    tail = lax.div(lax.div(p, nz) + (ny - 2), ny - 1)
    q = tail * (p - nz)
    k = lax.div(q, ny - 1)
    r = lax.rem(q, ny - 1)
    odd = lax.rem(k, 2)
    z = (1 - tail) * p + tail * (nz - 1 - k)
    y = tail * ((1 - odd) * (1 + r) + odd * (ny - 1 - r))
    return z * ny + y


def send_list(n):
    hops = n // 2
    split = n % 2 == 0

    def pieces(a, h):
        return [(a, h, 0)] if split and h == hops - 1 else [(a, h, 0), (a, h, 1)]

    ups = [p for h in range(1, hops) for p in pieces("u", h)]
    downs = [p for h in range(1, hops) for p in pieces("d", h)]
    own_u, own_d = pieces("u", 0), pieces("d", 0)
    return own_u + own_d[:1] + ups + own_d[1:] + downs


def gather_kernel(n_fs, n_tp, tokens, up_l, dn_l, up_w, dn_w, recv, x, hid, part, loc_sem, tok_s, tok_r, ring_s, ring_r, rs_s, rs_r):
    nz, ny = grid_of(n_fs)
    me_f, me_t = lax.axis_index("fs"), lax.axis_index("tp")
    pos = position_of(me_f, nz, ny)
    T, Dk = tokens.shape
    R, F = up_l.shape
    D = n_fs * R
    split_cols = (R // 2) % 128 == 0
    W = R // 2 if split_cols else R

    def at(offset):
        return index_at(lax.rem(pos + offset + n_fs, n_fs), nz, ny)

    right, left = at(1), at(-1)

    def tp_peer(k):
        return lax.rem(me_t + k, n_tp)

    barrier = pltpu.get_barrier_semaphore()
    for f in (right, left):
        pl.semaphore_signal(barrier, inc=1, device_id={"fs": f, "tp": me_t}, device_id_type=MESH)
    for k in range(1, n_tp):
        pl.semaphore_signal(barrier, inc=1, device_id={"fs": me_f, "tp": tp_peer(k)}, device_id_type=MESH)

    def up_piece(f, h):
        return up_w.at[pl.ds(pl.multiple_of(f * R + h * (R // 2), R // 2), R // 2), :]

    def dn_piece(f, h):
        if split_cols:
            return dn_w.at[:, pl.ds(pl.multiple_of(f * R + h * (R // 2), R // 2), R // 2)]
        return dn_w.at[pl.ds(h * (F // 2), F // 2), pl.ds(pl.multiple_of(f * R, R), R)]

    def tok_cols(t):
        return x.at[:, pl.ds(pl.multiple_of(t * Dk, Dk), Dk)]

    own = [
        pltpu.make_async_copy(up_l, up_w.at[pl.ds(pl.multiple_of(me_f * R, R), R), :], loc_sem.at[0]),
        pltpu.make_async_copy(dn_l, dn_w.at[:, pl.ds(pl.multiple_of(me_f * R, R), R)], loc_sem.at[1]),
        pltpu.make_async_copy(tokens, tok_cols(me_t), loc_sem.at[2]),
    ]
    for c in own:
        c.start()
    pl.semaphore_wait(barrier, n_tp + 1)

    order = send_list(n_fs)
    S = len(order)

    def ring_copy(s, d):
        a, hop, second = order[s]
        half = second if d == 0 else 1 - second
        f = at(-hop if d == 0 else hop)
        ref = up_piece(f, half) if a == "u" else dn_piece(f, half)
        return pltpu.make_async_remote_copy(
            src_ref=ref, dst_ref=ref, send_sem=ring_s.at[d, s], recv_sem=ring_r.at[d, s],
            device_id={"fs": right if d == 0 else left, "tp": me_t}, device_id_type=MESH,
        )

    def arrival(s, d):
        a, hop, second = order[s]
        half = second if d == 0 else 1 - second
        f = at(-(hop + 1) if d == 0 else hop + 1)
        return f, half, (up_piece(f, half) if a == "u" else dn_piece(f, half))

    def wait_arrival(s, d):
        f, half, ref = arrival(s, d)
        pltpu.make_async_remote_copy(
            src_ref=ref, dst_ref=ref, send_sem=ring_s.at[d, s], recv_sem=ring_r.at[d, s],
            device_id={"fs": right if d == 0 else left, "tp": me_t}, device_id_type=MESH,
        ).wait_recv()

    needs = [-1 if hop == 0 else order.index((a, hop - 1, second)) for a, hop, second in order]
    issued = [0]

    def issue(upto):
        while issued[0] < S and needs[issued[0]] <= upto:
            if upto < 0 and issued[0] >= 3:
                break
            for d in range(2):
                ring_copy(issued[0], d).start()
            issued[0] += 1

    own[0].wait()
    for d in range(2):
        ring_copy(0, d).start()
        ring_copy(1, d).start()
    own[2].wait()

    def token_copy(k):
        return pltpu.make_async_remote_copy(
            src_ref=tok_cols(me_t), dst_ref=tok_cols(me_t), send_sem=tok_s.at[k], recv_sem=tok_r.at[k],
            device_id={"fs": me_f, "tp": tp_peer(k)}, device_id_type=MESH,
        )

    for k in range(1, n_tp):
        token_copy(k).start()
    own[1].wait()
    issued[0] = 2
    issue(-1)

    def normalise():
        for k in range(1, n_tp):
            src = lax.rem(me_t - k + n_tp, n_tp)
            pltpu.make_async_remote_copy(
                src_ref=tok_cols(src), dst_ref=tok_cols(src), send_sem=tok_s.at[k], recv_sem=tok_r.at[k],
                device_id={"fs": me_f, "tp": tp_peer(k)}, device_id_type=MESH,
            ).wait_recv()
            token_copy(k).wait_send()
        rows = 64

        @pl.loop(0, T // rows)
        def _(i):
            r = pl.ds(pl.multiple_of(i * rows, rows), rows)
            v = x[r, :].astype(jnp.float32)
            x[r, :] = (v * lax.rsqrt(jnp.mean(v * v, axis=-1, keepdims=True) + norm_floor)).astype(jnp.bfloat16)

    def make_hidden():
        width = 256

        @pl.loop(0, F // width)
        def _(i):
            c = pl.ds(pl.multiple_of(i * width, width), width)
            pre = jnp.dot(x[...], up_w[:, c], preferred_element_type=jnp.float32)
            hid[:, c] = jnp.square(jnp.maximum(pre, 0.0)).astype(jnp.bfloat16)

    per_owner = Dk // W

    def part_copy(q):
        owner = lax.div(q, per_owner)
        local = lax.rem(q, per_owner)
        return owner, pltpu.make_async_remote_copy(
            src_ref=part.at[q],
            dst_ref=recv.at[me_t, :, pl.ds(pl.multiple_of(local * W, W), W)],
            send_sem=rs_s.at[q], recv_sem=rs_r.at[me_t, local],
            device_id={"fs": me_f, "tp": owner}, device_id_type=MESH,
        )

    def do_part(q):
        rows = T // 2
        owner, copy = part_copy(q)
        c = pl.ds(pl.multiple_of(q * W, W), W)

        @pl.loop(0, 2)
        def _(i):
            r = pl.ds(pl.multiple_of(i * rows, rows), rows)
            part[q, r, :] = jnp.dot(hid[r, :], dn_w[:, c], preferred_element_type=jnp.float32).astype(jnp.bfloat16)

        @pl.when(owner != me_t)
        def _():
            copy.start()

    ready = [me_f * (R // W) + h for h in range(R // W)]
    last_up = max(s for s in range(S) if order[s][0] == "u")
    norm_at = max(0, last_up - 2)
    for s in range(S):
        for d in range(2):
            wait_arrival(s, d)
        issue(s)
        if order[s][0] == "d" and split_cols:
            for d in range(2):
                f, half, _ = arrival(s, d)
                ready.append(f * 2 + half)
        if s == norm_at:
            normalise()
        if s == last_up:
            make_hidden()
        if s >= last_up:
            for q in ready:
                do_part(q)
            ready = []
    if not split_cols:
        @pl.loop(0, n_fs)
        def _(q):
            @pl.when(q != me_f)
            def _():
                do_part(q)

    keep = pl.ds(pl.multiple_of(0, W), W)

    @pl.loop(0, per_owner)
    def _(local):
        cols = pl.ds(pl.multiple_of(local * W, W), W)
        recv[me_t, :, cols] = part[me_t * per_owner + local]

    for d in range(2):
        for s in range(S):
            ring_copy(s, d).wait_send()

    @pl.loop(0, D // W)
    def _(q):
        owner, copy = part_copy(q)

        @pl.when(owner != me_t)
        def _():
            copy.wait_send()

    for k in range(1, n_tp):
        src = tp_peer(k)
        for local in range(per_owner):
            ref = recv.at[src, :, pl.ds(local * W, W)]
            pltpu.make_async_remote_copy(
                src_ref=ref, dst_ref=ref, send_sem=rs_s.at[0], recv_sem=rs_r.at[src, local],
                device_id={"fs": me_f, "tp": src}, device_id_type=MESH,
            ).wait_recv()


def finish_kernel(up_v, dn_v, recv, up_o, dn_o, mlp_o, total, sem):
    copies = [pltpu.make_async_copy(up_v, up_o, sem.at[0]), pltpu.make_async_copy(dn_v, dn_o, sem.at[1])]
    for c in copies:
        c.start()
    n, T, _ = recv.shape
    rows = 128

    @pl.loop(0, T // rows)
    def _(i):
        r = pl.ds(pl.multiple_of(i * rows, rows), rows)
        acc = recv[0, r, :].astype(jnp.float32)
        for k in range(1, n):
            acc += recv[k, r, :].astype(jnp.float32)
        total[r, :] = acc.astype(jnp.bfloat16)

    last = pltpu.make_async_copy(total, mlp_o, sem.at[2])
    last.start()
    for c in copies:
        c.wait()
    last.wait()


def solution(mesh):
    n_fs, n_tp = mesh.shape["fs"], mesh.shape["tp"]
    bf16 = jnp.bfloat16

    def on_device(tokens, norm_gain, up_master, down_master):
        up_l = (norm_gain[:, None] * up_master).astype(bf16)
        dn_l = jnp.transpose(down_master).astype(bf16)
        T, Dk = tokens.shape
        R, F = up_l.shape
        D = n_fs * R
        W = R // 2 if (R // 2) % 128 == 0 else R
        S = len(send_list(n_fs))
        any_spec = pl.BlockSpec(memory_space=pl.ANY)
        vmem_spec = pl.BlockSpec(memory_space=pltpu.VMEM)
        up_v, dn_v, recv = pl.pallas_call(
            functools.partial(gather_kernel, n_fs, n_tp),
            out_shape=(pltpu.VMEM((D, F), bf16), pltpu.VMEM((F, D), bf16), pltpu.VMEM((n_tp, T, Dk), bf16)),
            in_specs=[any_spec] * 3,
            out_specs=(vmem_spec,) * 3,
            scratch_shapes=[
                pltpu.VMEM((T, D), bf16),
                pltpu.VMEM((T, F), bf16),
                pltpu.VMEM((D // W, T, W), bf16),
                pltpu.SemaphoreType.DMA((3,)),
                pltpu.SemaphoreType.DMA((n_tp,)),
                pltpu.SemaphoreType.DMA((n_tp,)),
                pltpu.SemaphoreType.DMA((2, S)),
                pltpu.SemaphoreType.DMA((2, S)),
                pltpu.SemaphoreType.DMA((D // W,)),
                pltpu.SemaphoreType.DMA((n_tp, Dk // W)),
            ],
            compiler_params=pltpu.CompilerParams(
                collective_id=0, has_side_effects=True, vmem_limit_bytes=30 * 2**20
            ),
        )(tokens, up_l, dn_l)
        return pl.pallas_call(
            finish_kernel,
            out_shape=(
                jax.ShapeDtypeStruct((D, F), bf16),
                jax.ShapeDtypeStruct((F, D), bf16),
                jax.ShapeDtypeStruct((T, Dk), bf16),
            ),
            in_specs=[vmem_spec] * 3,
            out_specs=(any_spec,) * 3,
            scratch_shapes=[pltpu.VMEM((T, Dk), bf16), pltpu.SemaphoreType.DMA((3,))],
            compiler_params=pltpu.CompilerParams(vmem_limit_bytes=8 * 2**20),
        )(up_v, dn_v, recv)

    in_specs = (P("fs", "tp"), P("fs"), P("fs", "tp"), P("fs", "tp"))
    out_specs = (P(None, "tp"), P("tp", None), P("fs", "tp"))
    return jax.shard_map(on_device, mesh=mesh, in_specs=in_specs, out_specs=out_specs, check_vma=False)
```

time: 392 us -> 187 us (0.48)
  waiting for transfers between devices: 327 us -> 0 us
  Pallas kernels: 0 us -> 183 us
  matrix products: 25.7 us -> 0 us
  local copies, waits for them, and re-layouts: 19.4 us -> 1.77 us
  between operations: 13.8 us -> 0.67 us
  other arithmetic: 5.82 us -> 1.85 us
    all_gather x3 -> x0, waiting for transfers between devices: 283 us -> none  [the longest x1 126 us: on_device(): lax.all_gather(down_local, 'fs', axis=0, tiled=True)]
    pallas_call x0 -> x2, Pallas kernels: none -> 183 us  [the longest x1 176 us: on_device(): pl.pallas_call(functools.partial(gather_kernel, n_fs, n_tp), out_shape=(p...]
    reduce_scatter x1 -> x0, waiting for transfers between devices: 42.7 us -> none  [on_device(): lax.psum_scatter(partial_value.astype(jnp.bfloat16), 'tp', scatter_dimens...]
    dot_general x1 -> x0, matrix products: 25.7 us -> none  [on_device(): jnp.einsum('tf,df->td', hidden, down_whole, preferred_element_type=jnp.fl...]
    unnamed x3, local copies, waits for them, and re-layouts: 19.4 us -> 1.77 us
  transfers between devices with their start and end apart: 4 -> 0, of which waited for: 4 -> 0; matrix products, arithmetic and copies ran while one was open for 2% -> 0% of each run, Pallas kernels for 0% -> 0%
where the time goes in v1:
time: 187 us
  Pallas kernels  183 us (98%)
    pallas_call x1, Pallas kernels, on_device(): pl.pallas_call(functools.partial(gather_kernel, n_fs, n_tp), out_shape=(p...  176 us
    pallas_call x1, Pallas kernels, on_device(): pl.pallas_call(finish_kernel, out_shape=(jax.ShapeDtypeStruct((D, F), bf1...  6.28 us

profile of v1, /device:TPU:0, one launch (start us, length us, event | category | flops | bytes accessed | tf_op | source)
XLA Modules:
  0.0 186.9 jit_solution(14485348316005954869)
XLA Ops:
  0.6 0.0 copy-start
  0.6 1.9 multiply_convert_fusion.up_l
  2.5 1.8 copy.7
  4.3 0.0 copy-done
  4.3 176.3 %shard_map.67 = (bf16[2048,2048]{1,0:T(8,128)(2,1)S(1)}, bf16[2048,2048]{1,0:T(8,128)(2,1)S(1)}, bf16[4,1024,512]{2,1,0:T(8,128)(2,1)S(1)}) custom-call(bf16[1024,512]{1,0:T(8,128)(2,1)S(1)} %copy-done, bf16[256,2048]{1,0:T(8,128)(2,1)S(1)} %multiply_convert_fusion.up_l, bf16[2048,256]{1,0:T(8,128)(2,1)S(1)} %bitcast.3), custom_call_target="tpu_custom_call" | custom-call | tf_op jit(solution)/shard_map/pallas_call | solution.py:297
  180.6 6.3 %shard_map.68 = (bf16[2048,2048]{1,0:T(8,128)(2,1)}, bf16[2048,2048]{1,0:T(8,128)(2,1)}, bf16[1024,512]{1,0:T(8,128)(2,1)}) custom-call(bf16[2048,2048]{1,0:T(8,128)(2,1)S(1)} %get-tuple-element.6.up_v, bf16[2048,2048]{1,0:T(8,128)(2,1)S(1)} %get-tuple-element.7.dn_v, bf16[4,1024,512]{2,1,0:T(8,128)(2,1)S(1)} %get-tuple-element.8.recv), custom_call_target="tpu_custom_call" | custom-call | tf_op jit(solution)/shard_map/pallas_call | solution.py:318
Async XLA Ops:
  0.6 3.7 %copy-start = (bf16[1024,512]{1,0:T(8,128)(2,1)S(1)}, bf16[1024,512]{1,0:T(8,128)(2,1)}, u32[]{:S(2)}) copy-start(bf16[1024,512]{1,0:T(8,128)(2,1)} %tokens.1) | copy-start | bytes 3145732

commit v2 on v1

--- a/solution.py
+++ b/solution.py
@@ -53,7 +53,10 @@
     return own_u + own_d[:1] + ups + own_d[1:] + downs
 
 
-def gather_kernel(n_fs, n_tp, tokens, up_l, dn_l, up_w, dn_w, recv, x, hid, part, loc_sem, tok_s, tok_r, ring_s, ring_r, rs_s, rs_r):
+def gather_kernel(
+    n_fs, n_tp, tokens, gain, up_l, dn_l, up_w, dn_w, recv, x, hid, part, stage, up_f, dn_f, gain_v,
+    loc_sem, tok_s, tok_r, ring_s, ring_r, pre_s, pre_r, rs_s, rs_r,
+):
     nz, ny = grid_of(n_fs)
     me_f, me_t = lax.axis_index("fs"), lax.axis_index("tp")
     pos = position_of(me_f, nz, ny)
@@ -89,12 +92,21 @@
         return x.at[:, pl.ds(pl.multiple_of(t * Dk, Dk), Dk)]
 
     own = [
-        pltpu.make_async_copy(up_l, up_w.at[pl.ds(pl.multiple_of(me_f * R, R), R), :], loc_sem.at[0]),
-        pltpu.make_async_copy(dn_l, dn_w.at[:, pl.ds(pl.multiple_of(me_f * R, R), R)], loc_sem.at[1]),
-        pltpu.make_async_copy(tokens, tok_cols(me_t), loc_sem.at[2]),
+        pltpu.make_async_copy(up_l, up_f, loc_sem.at[0]),
+        pltpu.make_async_copy(tokens, tok_cols(me_t), loc_sem.at[1]),
+        pltpu.make_async_copy(dn_l, dn_f, loc_sem.at[2]),
     ]
-    for c in own:
+    gain_copy = pltpu.make_async_copy(gain, gain_v, loc_sem.at[3])
+    for c in [gain_copy] + own:
         c.start()
+    own_rows = pl.ds(pl.multiple_of(me_f * R, R), R)
+    gain_copy.wait()
+    spread = jnp.transpose(jnp.broadcast_to(gain_v[...], (128, R)))
+    own[0].wait()
+    for c in range(F // 128):
+        cols = pl.ds(c * 128, 128)
+        up_w[own_rows, cols] = (spread * up_f[:, cols]).astype(jnp.bfloat16)
+    own[1].wait()
     pl.semaphore_wait(barrier, n_tp + 1)
 
     order = send_list(n_fs)
@@ -134,11 +146,9 @@
                 ring_copy(issued[0], d).start()
             issued[0] += 1
 
-    own[0].wait()
-    for d in range(2):
-        ring_copy(0, d).start()
-        ring_copy(1, d).start()
-    own[2].wait()
+    for s in range(2):
+        for d in range(2):
+            ring_copy(s, d).start()
 
     def token_copy(k):
         return pltpu.make_async_remote_copy(
@@ -148,7 +158,14 @@
 
     for k in range(1, n_tp):
         token_copy(k).start()
-    own[1].wait()
+    own[2].wait()
+    block = min(F, 256)
+
+    @pl.loop(0, F // block)
+    def _(i):
+        r = pl.ds(pl.multiple_of(i * block, block), block)
+        dn_w[r, own_rows] = jnp.transpose(dn_f[:, r]).astype(jnp.bfloat16)
+
     issued[0] = 2
     issue(-1)
 
@@ -178,63 +195,109 @@
             hid[:, c] = jnp.square(jnp.maximum(pre, 0.0)).astype(jnp.bfloat16)
 
     per_owner = Dk // W
-
-    def part_copy(q):
+    nx = n_tp // 2
+    half_rows = T // 2
+    me_x, me_c = lax.div(me_t, 2), lax.rem(me_t, 2)
+    sibling = me_t + 1 - 2 * me_c
+    my_half = pl.ds(pl.multiple_of(me_c * half_rows, half_rows), half_rows)
+    its_half = pl.ds(pl.multiple_of((1 - me_c) * half_rows, half_rows), half_rows)
+
+    def device(t):
+        return dict(device_id={"fs": me_f, "tp": t}, device_id_type=MESH)
+
+    def cols_of(q):
+        return pl.ds(pl.multiple_of(lax.rem(q, per_owner) * W, W), W)
+
+    def whole_copy(q):
+        return pltpu.make_async_remote_copy(
+            src_ref=part.at[q], dst_ref=recv.at[nx, :, cols_of(q)],
+            send_sem=rs_s.at[q], recv_sem=rs_r.at[nx, lax.rem(q, per_owner), 0], **device(sibling),
+        )
+
+    def pair_copy(q):
+        return pltpu.make_async_remote_copy(
+            src_ref=part.at[q, its_half], dst_ref=stage.at[q],
+            send_sem=pre_s.at[q], recv_sem=pre_r.at[q], **device(sibling),
+        )
+
+    def half_copy(q):
+        return pltpu.make_async_remote_copy(
+            src_ref=part.at[q, my_half], dst_ref=recv.at[me_x, my_half, cols_of(q)],
+            send_sem=rs_s.at[q], recv_sem=rs_r.at[me_x, lax.rem(q, per_owner), me_c],
+            **device(lax.div(q, per_owner)),
+        )
+
+    def share(q):
         owner = lax.div(q, per_owner)
-        local = lax.rem(q, per_owner)
-        return owner, pltpu.make_async_remote_copy(
-            src_ref=part.at[q],
-            dst_ref=recv.at[me_t, :, pl.ds(pl.multiple_of(local * W, W), W)],
-            send_sem=rs_s.at[q], recv_sem=rs_r.at[me_t, local],
-            device_id={"fs": me_f, "tp": owner}, device_id_type=MESH,
-        )
-
-    def do_part(q):
-        rows = T // 2
-        owner, copy = part_copy(q)
-        c = pl.ds(pl.multiple_of(q * W, W), W)
+
+        @pl.when(owner == sibling)
+        def _():
+            whole_copy(q).start()
+
+        @pl.when(lax.div(owner, 2) != me_x)
+        def _():
+            pair_copy(q).start()
+
+    def pass_on(q):
+        @pl.when(lax.div(q, 2 * per_owner) != me_x)
+        def _():
+            pair_copy(q).wait_recv()
+            both = part[q, my_half, :].astype(jnp.float32) + stage[q].astype(jnp.float32)
+            part[q, my_half, :] = both.astype(jnp.bfloat16)
+            half_copy(q).start()
+
+    def do_parts(first, count):
+        c = pl.ds(pl.multiple_of(first * W, W), count * W)
 
         @pl.loop(0, 2)
         def _(i):
-            r = pl.ds(pl.multiple_of(i * rows, rows), rows)
-            part[q, r, :] = jnp.dot(hid[r, :], dn_w[:, c], preferred_element_type=jnp.float32).astype(jnp.bfloat16)
-
-        @pl.when(owner != me_t)
-        def _():
-            copy.start()
-
-    ready = [me_f * (R // W) + h for h in range(R // W)]
+            r = pl.ds(pl.multiple_of(i * half_rows, half_rows), half_rows)
+            out = jnp.dot(hid[r, :], dn_w[:, c], preferred_element_type=jnp.float32).astype(jnp.bfloat16)
+            for k in range(count):
+                part[first + k, r, :] = out[:, k * W : (k + 1) * W]
+
+        for k in range(count):
+            share(first + k)
+
+    per_chunk = R // W
+    ready = [(me_f * per_chunk, per_chunk)]
     last_up = max(s for s in range(S) if order[s][0] == "u")
     norm_at = max(0, last_up - 2)
     for s in range(S):
         for d in range(2):
             wait_arrival(s, d)
         issue(s)
-        if order[s][0] == "d" and split_cols:
-            for d in range(2):
-                f, half, _ = arrival(s, d)
-                ready.append(f * 2 + half)
+        a, hop, _ = order[s]
+        if a == "d" and split_cols:
+            if n_fs % 2 == 0 and hop == n_fs // 2 - 1:
+                ready.append((at(hop + 1) * 2, 2))
+            else:
+                for d in range(2):
+                    f, half, _ = arrival(s, d)
+                    ready.append((f * 2 + half, 1))
         if s == norm_at:
             normalise()
         if s == last_up:
             make_hidden()
         if s >= last_up:
-            for q in ready:
-                do_part(q)
+            for first, count in ready:
+                do_parts(first, count)
+            for first, count in ready:
+                for k in range(count):
+                    pass_on(first + k)
             ready = []
     if not split_cols:
         @pl.loop(0, n_fs)
         def _(q):
             @pl.when(q != me_f)
             def _():
-                do_part(q)
-
-    keep = pl.ds(pl.multiple_of(0, W), W)
+                do_parts(q, 1)
+                pass_on(q)
 
     @pl.loop(0, per_owner)
     def _(local):
         cols = pl.ds(pl.multiple_of(local * W, W), W)
-        recv[me_t, :, cols] = part[me_t * per_owner + local]
+        recv[me_x, :, cols] = part[me_t * per_owner + local]
 
     for d in range(2):
         for s in range(S):
@@ -242,20 +305,27 @@
 
     @pl.loop(0, D // W)
     def _(q):
-        owner, copy = part_copy(q)
-
-        @pl.when(owner != me_t)
+        owner = lax.div(q, per_owner)
+
+        @pl.when(owner == sibling)
         def _():
-            copy.wait_send()
-
-    for k in range(1, n_tp):
-        src = tp_peer(k)
-        for local in range(per_owner):
-            ref = recv.at[src, :, pl.ds(local * W, W)]
-            pltpu.make_async_remote_copy(
-                src_ref=ref, dst_ref=ref, send_sem=rs_s.at[0], recv_sem=rs_r.at[src, local],
-                device_id={"fs": me_f, "tp": src}, device_id_type=MESH,
-            ).wait_recv()
+            whole_copy(q).wait_send()
+
+        @pl.when(lax.div(owner, 2) != me_x)
+        def _():
+            pair_copy(q).wait_send()
+            half_copy(q).wait_send()
+
+    for local in range(per_owner):
+        q = me_t * per_owner + local
+        whole_copy(q).wait_recv()
+        for k in range(1, nx):
+            src = lax.rem(me_x + k, nx)
+            for c in range(2):
+                ref = recv.at[src, pl.ds(c * half_rows, half_rows), pl.ds(local * W, W)]
+                pltpu.make_async_remote_copy(
+                    src_ref=ref, dst_ref=ref, send_sem=rs_s.at[0], recv_sem=rs_r.at[src, local, c], **device(sibling),
+                ).wait_recv()
 
 
 def finish_kernel(up_v, dn_v, recv, up_o, dn_o, mlp_o, total, sem):
@@ -285,10 +355,8 @@
     bf16 = jnp.bfloat16
 
     def on_device(tokens, norm_gain, up_master, down_master):
-        up_l = (norm_gain[:, None] * up_master).astype(bf16)
-        dn_l = jnp.transpose(down_master).astype(bf16)
         T, Dk = tokens.shape
-        R, F = up_l.shape
+        R, F = up_master.shape
         D = n_fs * R
         W = R // 2 if (R // 2) % 128 == 0 else R
         S = len(send_list(n_fs))
@@ -296,25 +364,31 @@
         vmem_spec = pl.BlockSpec(memory_space=pltpu.VMEM)
         up_v, dn_v, recv = pl.pallas_call(
             functools.partial(gather_kernel, n_fs, n_tp),
-            out_shape=(pltpu.VMEM((D, F), bf16), pltpu.VMEM((F, D), bf16), pltpu.VMEM((n_tp, T, Dk), bf16)),
-            in_specs=[any_spec] * 3,
+            out_shape=(pltpu.VMEM((D, F), bf16), pltpu.VMEM((F, D), bf16), pltpu.VMEM((n_tp // 2 + 1, T, Dk), bf16)),
+            in_specs=[pl.BlockSpec(memory_space=pltpu.HBM)] * 4,
             out_specs=(vmem_spec,) * 3,
             scratch_shapes=[
                 pltpu.VMEM((T, D), bf16),
                 pltpu.VMEM((T, F), bf16),
                 pltpu.VMEM((D // W, T, W), bf16),
-                pltpu.SemaphoreType.DMA((3,)),
+                pltpu.VMEM((D // W, T // 2, W), bf16),
+                pltpu.VMEM((R, F), jnp.float32),
+                pltpu.VMEM((R, F), jnp.float32),
+                pltpu.VMEM((1, R), jnp.float32),
+                pltpu.SemaphoreType.DMA((4,)),
                 pltpu.SemaphoreType.DMA((n_tp,)),
                 pltpu.SemaphoreType.DMA((n_tp,)),
                 pltpu.SemaphoreType.DMA((2, S)),
                 pltpu.SemaphoreType.DMA((2, S)),
                 pltpu.SemaphoreType.DMA((D // W,)),
-                pltpu.SemaphoreType.DMA((n_tp, Dk // W)),
+                pltpu.SemaphoreType.DMA((D // W,)),
+                pltpu.SemaphoreType.DMA((D // W,)),
+                pltpu.SemaphoreType.DMA((n_tp // 2 + 1, Dk // W, 2)),
             ],
             compiler_params=pltpu.CompilerParams(
-                collective_id=0, has_side_effects=True, vmem_limit_bytes=30 * 2**20
+                collective_id=0, has_side_effects=True, vmem_limit_bytes=44 * 2**20
             ),
-        )(tokens, up_l, dn_l)
+        )(tokens, norm_gain[None, :], up_master, down_master)
         return pl.pallas_call(
             finish_kernel,
             out_shape=(

time: 187 us -> 180 us (0.963)
  Pallas kernels: 183 us -> 178 us
    pallas_call x1, Pallas kernels: 176 us -> 172 us  [on_device(): pl.pallas_call(functools.partial(gather_kernel, n_fs, n_tp), out_shape=(p...]
where the time goes in v2:
time: 180 us; the launch traced here: 179 us
  Pallas kernels  178 us (99%)
    pallas_call x1, Pallas kernels, on_device(): pl.pallas_call(functools.partial(gather_kernel, n_fs, n_tp), out_shape=(p...  172 us
    pallas_call x1, Pallas kernels, on_device(): pl.pallas_call(finish_kernel, out_shape=(jax.ShapeDtypeStruct((D, F), bf1...  6.28 us

profile of v2, /device:TPU:0, one launch (start us, length us, event | category | flops | bytes accessed | tf_op | source)
XLA Modules:
  0.0 178.9 jit_solution(3934451807882865767)
XLA Ops:
  0.6 172.0 %shard_map.67 = (bf16[2048,2048]{1,0:T(8,128)(2,1)S(1)}, bf16[2048,2048]{1,0:T(8,128)(2,1)S(1)}, bf16[3,1024,512]{2,1,0:T(8,128)(2,1)S(1)}) custom-call(bf16[1024,512]{1,0:T(8,128)(2,1)} %tokens.1, f32[1,256]{1,0:T(1,128)} %bitcast.1, f32[256,2048]{1,0:T(8,128)} %up_l.1, f32[256,2048]{1,0:T(8,128)} %dn_l.1), custom_call_target="tpu_custom_call" | custom-call | tf_op jit(solution)/shard_map/pallas_call | solution.py:365
  172.6 6.3 %shard_map.68 = (bf16[2048,2048]{1,0:T(8,128)(2,1)}, bf16[2048,2048]{1,0:T(8,128)(2,1)}, bf16[1024,512]{1,0:T(8,128)(2,1)}) custom-call(bf16[2048,2048]{1,0:T(8,128)(2,1)S(1)} %get-tuple-element.6.up_v, bf16[2048,2048]{1,0:T(8,128)(2,1)S(1)} %get-tuple-element.7.dn_v, bf16[3,1024,512]{2,1,0:T(8,128)(2,1)S(1)} %get-tuple-element.8.recv), custom_call_target="tpu_custom_call" | custom-call | tf_op jit(solution)/shard_map/pallas_call | solution.py:392

commit v3 on v2

--- a/solution.py
+++ b/solution.py
@@ -227,17 +227,6 @@
             **device(lax.div(q, per_owner)),
         )
 
-    def share(q):
-        owner = lax.div(q, per_owner)
-
-        @pl.when(owner == sibling)
-        def _():
-            whole_copy(q).start()
-
-        @pl.when(lax.div(owner, 2) != me_x)
-        def _():
-            pair_copy(q).start()
-
     def pass_on(q):
         @pl.when(lax.div(q, 2 * per_owner) != me_x)
         def _():
@@ -251,13 +240,20 @@
 
         @pl.loop(0, 2)
         def _(i):
-            r = pl.ds(pl.multiple_of(i * half_rows, half_rows), half_rows)
+            r = pl.ds(pl.multiple_of(lax.rem(i + 1 + me_c, 2) * half_rows, half_rows), half_rows)
             out = jnp.dot(hid[r, :], dn_w[:, c], preferred_element_type=jnp.float32).astype(jnp.bfloat16)
             for k in range(count):
                 part[first + k, r, :] = out[:, k * W : (k + 1) * W]
-
-        for k in range(count):
-            share(first + k)
+            for k in range(count):
+                owner = lax.div(first + k, per_owner)
+
+                @pl.when((i == 0) & (lax.div(owner, 2) != me_x))
+                def _():
+                    pair_copy(first + k).start()
+
+                @pl.when((i == 1) & (owner == sibling))
+                def _():
+                    whole_copy(first + k).start()
 
     per_chunk = R // W
     ready = [(me_f * per_chunk, per_chunk)]

time: 180 us -> 180 us (level)
  no operation moved by 1% of the time
where the time goes in v3:
time: 180 us; the launch traced here: 179 us
  Pallas kernels  179 us (99%)
    pallas_call x1, Pallas kernels, on_device(): pl.pallas_call(functools.partial(gather_kernel, n_fs, n_tp), out_shape=(p...  172 us
    pallas_call x1, Pallas kernels, on_device(): pl.pallas_call(finish_kernel, out_shape=(jax.ShapeDtypeStruct((D, F), bf1...  6.28 us

profile of v3, /device:TPU:0, one launch (start us, length us, event | category | flops | bytes accessed | tf_op | source)
XLA Modules:
  0.0 179.3 jit_solution(17146898356240857918)
XLA Ops:
  0.6 172.4 %shard_map.67 = (bf16[2048,2048]{1,0:T(8,128)(2,1)S(1)}, bf16[2048,2048]{1,0:T(8,128)(2,1)S(1)}, bf16[3,1024,512]{2,1,0:T(8,128)(2,1)S(1)}) custom-call(bf16[1024,512]{1,0:T(8,128)(2,1)} %tokens.1, f32[1,256]{1,0:T(1,128)} %bitcast.1, f32[256,2048]{1,0:T(8,128)} %up_l.1, f32[256,2048]{1,0:T(8,128)} %dn_l.1), custom_call_target="tpu_custom_call" | custom-call | tf_op jit(solution)/shard_map/pallas_call | solution.py:361
  173.0 6.3 %shard_map.68 = (bf16[2048,2048]{1,0:T(8,128)(2,1)}, bf16[2048,2048]{1,0:T(8,128)(2,1)}, bf16[1024,512]{1,0:T(8,128)(2,1)}) custom-call(bf16[2048,2048]{1,0:T(8,128)(2,1)S(1)} %get-tuple-element.6.up_v, bf16[2048,2048]{1,0:T(8,128)(2,1)S(1)} %get-tuple-element.7.dn_v, bf16[3,1024,512]{2,1,0:T(8,128)(2,1)S(1)} %get-tuple-element.8.recv), custom_call_target="tpu_custom_call" | custom-call | tf_op jit(solution)/shard_map/pallas_call | solution.py:388
